TPU v7x, 128 devices: a whole 4x4x4 slice. The times are simulated.
128 devices in a mesh: ep: 64 (over z, y, x), tp: 2 (over core).
Axes of the slice: x: 4, y: 4, z: 4, core: 2. Of those that a mesh axis runs over, the one named last changes fastest.
Arguments:
- tokens: bfloat16 [1024, 2048], P('ep'), may hold values from -6 to 6
- norm_gain: float32 [2048], replicated, may hold values from 0.1 to 1.9
- query_weight: bfloat16 [2048, 1024], P('ep', 'tp'), may hold values from -0.125 to 0.125
- key_weight: bfloat16 [2048, 1024], P('ep', 'tp'), may hold values from -0.125 to 0.125
- value_weight: bfloat16 [2048, 1024], P('ep', 'tp'), may hold values from -0.125 to 0.125
- outgate_weight: bfloat16 [2048, 1024], P('ep', 'tp'), may hold values from -0.125 to 0.125
- input_weight: bfloat16 [2048, 8], P('ep', 'tp'), may hold values from -0.125 to 0.125
- forget_weight: bfloat16 [2048, 8], P('ep', 'tp'), may hold values from -0.125 to 0.125
- forget_bias: float32 [8], P('tp'), may hold values from -1 to 5
- memory: float32 [1024, 8, 128, 128], P('ep', 'tp'), may hold values from -2.4 to 2.4
- stabilizer: float32 [1024, 8], P('ep', 'tp'), may hold values from -3 to 3
- head_gain: float32 [1024], P('tp'), may hold values from 0.1 to 1.9
- mix_weight: bfloat16 [1024, 2048], P('tp', 'ep'), may hold values from -0.1875 to 0.1875
- second_gain: float32 [2048], replicated, may hold values from 0.1 to 1.9
- route_experts: int32 [1024, 4], P('ep'), may hold values from 0 to 63, all different within a row; in each aligned block of 16 rows (0 to 15, 16 to 31, ...) at most 2 rows name the same one
- route_weight: float32 [1024, 4], P('ep'), may hold values from 0.1 to 1
- expert_gate: bfloat16 [64, 2048, 2048], P('ep', None, 'tp'), may hold values from -0.5 to 0.5
- expert_up: bfloat16 [64, 2048, 2048], P('ep', None, 'tp'), may hold values from -0.5 to 0.5
- expert_down: bfloat16 [64, 2048, 2048], P('ep', 'tp'), may hold values from -0.03125 to 0.03125
- dense_gate: bfloat16 [4096, 2048], P(('ep', 'tp')), may hold values from -0.125 to 0.125
- dense_up: bfloat16 [4096, 2048], P(('ep', 'tp')), may hold values from -0.125 to 0.125
- dense_down: bfloat16 [4096, 2048], P(('ep', 'tp')), may hold values from -0.09375 to 0.09375
- branch_scale: float32 [2048], replicated, may hold values from 0.3 to 1.5
Outputs:
- mixed: bfloat16 [1024, 2048], P('ep', 'tp')
- memory_new: float32 [1024, 8, 128, 128], P('ep', 'tp')
- stabilizer_new: float32 [1024, 8], P('ep', 'tp')
Inputs may be any that keep to these rules, and one draw needn't show every extreme that they name: `route_experts`: each row names 4 different experts. Within each aligned block of 16 rows no expert is named by more than 2 rows, and in every draw some expert is named by exactly 2 rows of some block.
All inputs are finite; a program needn't handle non-finite values.
Results may differ from a plain program's by a relative error of at most 0.03.
Values may be sent and summed in bfloat16 or wider, within the bound.
A program may use at most 128 MiB of HBM per device.

v0:
```python
import jax
import jax.numpy as jnp
from jax import lax
from jax.sharding import PartitionSpec as P

norm_eps = 1e-05
clamp_limit = 7.0
sigmoid_slope = 1.702


def in_one_piece(arrays, axis, dim, along):
    widths = [a.shape[along] for a in arrays]
    both = jnp.concatenate(arrays, axis=along)
    whole = lax.all_gather(both, axis, axis=dim, tiled=True)
    return tuple(jnp.split(whole, [sum(widths[:k]) for k in range(1, len(widths))], axis=along))


def sent_to_all(shard, axis):
    devices = lax.axis_size(axis)
    return lax.all_to_all(
        jnp.broadcast_to(shard[None], (devices, *shard.shape)), axis, 0, 0, tiled=True
    )


def taken_together(shard, axis):
    return sent_to_all(shard, axis).astype(jnp.float32).sum(axis=0)


def cut_along(shard, dim, devices):
    lengths = shard.shape
    pieces = shard.reshape(*lengths[:dim], devices, lengths[dim] // devices, *lengths[dim + 1 :])
    return jnp.moveaxis(pieces, dim, 0)


def sent_and_summed(shard, axis, dim):
    devices = lax.axis_size(axis)
    pieces = lax.all_to_all(cut_along(shard, dim, devices), axis, 0, 0, tiled=True)
    return jnp.sum(pieces.astype(jnp.float32), axis=0)


def rms_scale(values, gain):
    mean_square = jnp.mean(values * values, axis=-1, keepdims=True)
    return values * lax.rsqrt(mean_square + norm_eps) * gain


def round_half(values):
    return lax.optimization_barrier(values.astype(jnp.bfloat16)).astype(jnp.float32)


def clamped_unit(gate_pre, up_pre):
    gate_clamped = jnp.minimum(gate_pre, clamp_limit)
    up_clamped = jnp.clip(up_pre, -clamp_limit, clamp_limit)
    return (
        (up_clamped + 1.0) * gate_clamped * jax.nn.sigmoid(sigmoid_slope * gate_clamped)
    ).astype(jnp.bfloat16)


def memory_step(projected, forget_bias, memory, stabilizer, head_gain):
    query_rows, key_rows, value_rows, outgate_rows, input_pre, forget_pre = projected
    sequences, head_count = stabilizer.shape
    head_size = memory.shape[-1]
    log_forget = jax.nn.log_sigmoid(forget_pre + forget_bias)
    stab_new = jnp.maximum(log_forget + stabilizer, input_pre)
    carried = jnp.exp(log_forget + stabilizer - stab_new)
    written = jnp.exp(input_pre - stab_new)
    query_heads = query_rows.astype(jnp.float32).reshape(sequences, head_count, head_size)
    key_heads = key_rows.astype(jnp.float32).reshape(
        sequences, head_count, head_size
    ) * head_size ** (-0.5)
    value_heads = value_rows.astype(jnp.float32).reshape(sequences, head_count, head_size)
    memory_new = (
        carried[:, :, None, None] * memory
        + written[:, :, None, None] * value_heads[:, :, :, None] * key_heads[:, :, None, :]
    )
    readout = jnp.einsum("bhvk,bhk->bhv", memory_new, query_heads)
    out_gate = jax.nn.sigmoid(
        outgate_rows.astype(jnp.float32).reshape(sequences, head_count, head_size)
    )
    gated = (rms_scale(readout, head_gain.reshape(head_count, head_size)) * out_gate).astype(
        jnp.bfloat16
    )
    return (gated.reshape(sequences, head_count * head_size), memory_new, stab_new)


def expert_apply(rows, gate_weight, up_weight, down_weight):
    gate_pre = jnp.dot(rows, gate_weight, preferred_element_type=jnp.float32)
    up_pre = jnp.dot(rows, up_weight, preferred_element_type=jnp.float32)
    activity = clamped_unit(gate_pre, up_pre)
    return jnp.dot(activity, down_weight, preferred_element_type=jnp.float32).astype(jnp.bfloat16)


def slot_table(hit_mask, capacity):
    ranks = jnp.cumsum(hit_mask, axis=1) - 1.0
    slots = jnp.arange(capacity).astype(jnp.float32)
    return hit_mask[:, None, :] * (ranks[:, None, :] == slots[None, :, None]).astype(jnp.float32)


def body(
    tokens,
    norm_gain,
    query_weight,
    key_weight,
    value_weight,
    outgate_weight,
    input_weight,
    forget_weight,
    forget_bias,
    memory,
    stabilizer,
    head_gain,
    mix_weight,
    second_gain,
    route_experts,
    route_weight,
    expert_gate,
    expert_up,
    expert_down,
    dense_gate,
    dense_up,
    dense_down,
    branch_scale,
):
    sequences, model_width = tokens.shape
    ep_count = lax.axis_size("ep")
    tp_count = lax.axis_size("tp")
    part_width = model_width // tp_count
    top_count = route_experts.shape[1]
    expert_count = expert_gate.shape[0] * ep_count
    capacity = max(2, 2 * sequences * top_count // expert_count)
    inputs_float = tokens.astype(jnp.float32)
    normed = rms_scale(inputs_float, norm_gain).astype(jnp.bfloat16)
    pieces = in_one_piece(
        (query_weight, key_weight, value_weight, outgate_weight, input_weight, forget_weight),
        "ep",
        0,
        1,
    )
    sums = tuple((jnp.dot(normed, piece, preferred_element_type=jnp.float32) for piece in pieces))
    projected = (
        sums[0].astype(jnp.bfloat16),
        sums[1].astype(jnp.bfloat16),
        sums[2].astype(jnp.bfloat16),
        sums[3].astype(jnp.bfloat16),
        sums[4],
        sums[5],
    )
    gated, memory_new, stab_new = memory_step(projected, forget_bias, memory, stabilizer, head_gain)
    partial_value = jnp.dot(
        gated,
        lax.all_gather(mix_weight, "ep", axis=1, tiled=True),
        preferred_element_type=jnp.float32,
    )
    attended = taken_together(round_half(partial_value).astype(jnp.bfloat16), "tp").astype(
        jnp.float32
    )
    residual = (inputs_float + attended).astype(jnp.bfloat16)
    residual_float = residual.astype(jnp.float32)
    normed_second = rms_scale(residual_float, second_gain).astype(jnp.bfloat16)
    own_residual = lax.dynamic_slice_in_dim(
        residual_float, lax.axis_index("tp") * part_width, part_width, 1
    )
    own_scale = lax.dynamic_slice_in_dim(
        branch_scale, lax.axis_index("tp") * part_width, part_width, 0
    )
    matched = route_experts[:, :, None] == jnp.arange(expert_count)[None, None, :]
    hit_mask = jnp.any(matched, axis=1).astype(jnp.float32).T
    weights = jnp.sum(jnp.where(matched, route_weight[:, :, None], 0.0), axis=1).T
    select = slot_table(hit_mask, capacity)
    outgoing = jnp.einsum(
        "ecs,sd->ecd",
        select.astype(jnp.bfloat16),
        normed_second,
        preferred_element_type=jnp.float32,
    ).astype(jnp.bfloat16)
    received = lax.all_to_all(outgoing, "ep", split_axis=0, concat_axis=0, tiled=True)
    count = received.shape[1]
    partial_out = expert_apply(
        received.reshape(-1, model_width), expert_gate[0], expert_up[0], expert_down[0]
    )
    halves = sent_and_summed(partial_out.astype(jnp.float32).astype(jnp.bfloat16), "tp", 1)
    returned = lax.all_to_all(
        halves.reshape(ep_count, count, part_width).astype(jnp.bfloat16),
        "ep",
        split_axis=0,
        concat_axis=0,
        tiled=True,
    ).astype(jnp.float32)
    routed = jnp.einsum("ecs,ecd->sd", select * weights[:, None, :], returned)
    gate_piece, up_piece, down_piece = in_one_piece((dense_gate, dense_up, dense_down), "ep", 0, 1)
    gate_rows = jnp.einsum(
        "td,fd->tf", normed_second, gate_piece, preferred_element_type=jnp.float32
    )
    lift_rows = jnp.einsum("td,fd->tf", normed_second, up_piece, preferred_element_type=jnp.float32)
    activity = (jax.nn.silu(gate_rows) * lift_rows).astype(jnp.bfloat16)
    total = jnp.dot(activity, down_piece, preferred_element_type=jnp.float32)
    halves = sent_and_summed(total.astype(jnp.bfloat16), "tp", 1)
    branch = halves * own_scale
    mixed = own_residual + routed + branch
    return (mixed.astype(jnp.bfloat16), memory_new, stab_new)


def solution(mesh):
    in_specs = (
        P("ep", None),
        P(),
        P("ep", "tp"),
        P("ep", "tp"),
        P("ep", "tp"),
        P("ep", "tp"),
        P("ep", "tp"),
        P("ep", "tp"),
        P("tp"),
        P("ep", "tp", None, None),
        P("ep", "tp"),
        P("tp"),
        P("tp", "ep"),
        P(),
        P("ep", None),
        P("ep", None),
        P("ep", None, "tp"),
        P("ep", None, "tp"),
        P("ep", "tp", None),
        P(("ep", "tp"), None),
        P(("ep", "tp"), None),
        P(("ep", "tp"), None),
        P(),
    )
    out_specs = (P("ep", "tp"), P("ep", "tp", None, None), P("ep", "tp"))
    return jax.shard_map(body, mesh=mesh, in_specs=in_specs, out_specs=out_specs, check_vma=False)
```

profile of v0, /device:TPU:0, one launch (start us, length us, event | category | flops | bytes accessed | tf_op | source)
XLA Modules:
  0.0 342.2 jit_solution(8388457338373234706)
XLA Ops:
  8.8 1.5 concatenate.6
  11.2 1.8 pad_maximum_fusion
  15.1 78.9 %all-gather.4.cloned.1.call-done = bf16[2048,2056]{1,0:T(8,128)(2,1)} async-done(((bf16[32,2056]{1,0:T(8,128)(2,1)}), bf16[2048,2056]{1,0:T(8,128)(2,1)}) %all-gather.4.cloned.1.call-update) | async-done | bytes 8421392 | tf_op jit(solution)/shard_map/all_gather | solution.py:14
  94.0 1.3 fusion.94
  95.3 1.8 subtract_exponential_fusion.1
  97.2 2.1 fusion.58
  99.4 2.0 fusion.67
  101.4 2.0 fusion.70
  103.4 2.0 fusion.88
  105.6 3.1 multiply_add_fusion
  108.7 2.0 copy-done
  112.1 49.8 %all-gather.6.cloned.1.call-done = bf16[512,2048]{0,1:T(8,128)(2,1)} async-done(((bf16[512,32]{0,1:T(8,128)(2,1)}), bf16[512,2048]{0,1:T(8,128)(2,1)}) %all-gather.6.cloned.1.call-update) | async-done | bytes 2097168 | tf_op jit(solution)/shard_map/all_gather | solution.py:150
  161.8 2.2 convolution_convert_fusion.1
  164.1 3.8 %all_to_all.25 = bf16[2,16,2048]{2,1,0:T(8,128)(2,1)S(1)} all-to-all(bf16[2,16,2048]{2,1,0:T(8,128)(2,1)S(1)} %broadcast_in_dim.10), channel_id=1, replica_groups=mesh['ep'=64,'tp'=2] {'tp'}, dimensions={0} | all-to-all | bytes 262144 | tf_op jit(solution)/shard_map/all_to_all | solution.py:20
  169.2 22.5 %all_to_all.26 = bf16[64,2,2048]{2,1,0:T(2,128)(2,1)S(1)} all-to-all(bf16[64,2,2048]{2,1,0:T(2,128)(2,1)S(1)} %copy.62), channel_id=1, replica_groups=mesh['ep'=64,'tp'=2] {'ep'}, dimensions={0} | all-to-all | bytes 1048576 | tf_op jit(solution)/shard_map/all_to_all | solution.py:175
  191.9 2.9 fusion.37
  194.8 5.5 %fusion.12 = bf16[128,2048]{1,0:T(8,128)(2,1)S(1)} fusion(bf16[1,1024,2048]{2,1,0:T(8,128)(2,1)} %param.41, f32[128,1024]{1,0:T(8,128)S(1)} %fusion.37, bf16[128,2048]{1,0:T(8,128)(2,1)S(1)} %reshape.97, bf16[1,2048,1024]{2,1,0:T(8,128)(2,1)} %param.40), kind=kOutput, calls=%fused_computation.13 | convolution fusion | flops 1075183616 | bytes 9961472 | tf_op jit(solution)/shard_map/dot_general | solution.py:89
  200.4 4.2 %all_to_all.27 = bf16[2,128,1024]{2,1,0:T(8,128)(2,1)S(1)} all-to-all(bf16[2,128,1024]{2,1,0:T(8,128)(2,1)S(1)} %bitcast.67), channel_id=1, replica_groups=mesh['ep'=64,'tp'=2] {'tp'}, dimensions={0} | all-to-all | bytes 1048576 | tf_op jit(solution)/shard_map/all_to_all | solution.py:37
  205.4 91.2 %all-gather.8.cloned.1.call-done = bf16[2048,6144]{1,0:T(8,128)(2,1)} async-done(((bf16[32,6144]{1,0:T(8,128)(2,1)}), bf16[2048,6144]{1,0:T(8,128)(2,1)}) %all-gather.8.cloned.1.call-update) | async-done | bytes 25165840 | tf_op jit(solution)/shard_map/all_gather | solution.py:14
  296.6 5.6 %fusion.4 = f32[16,2048]{1,0:T(8,128)S(1)} fusion(bf16[16,2048]{1,0:T(8,128)(2,1)S(1)} %multiply_convert_fusion, bf16[2048,6144]{1,0:T(8,128)(2,1)} %all-gather.8.cloned.1.call-done), kind=kOutput, calls=%fused_computation.4 | convolution fusion | flops 134217728 | bytes 8585216 | tf_op jit(solution)/shard_map/td,fd->tf/dot_general | solution.py:190
  302.3 9.2 %fusion.21 = bf16[16,2048]{1,0:T(8,128)(2,1)S(1)} fusion(bf16[2048,6144]{1,0:T(8,128)(2,1)} %all-gather.8.cloned.1.call-done, bf16[16,2048]{1,0:T(8,128)(2,1)S(1)} %multiply_convert_fusion, f32[16,2048]{1,0:T(8,128)S(1)} %fusion.4), kind=kOutput, calls=%fused_computation.17 | convolution fusion | flops 268664832 | bytes 17039360 | tf_op jit(solution)/shard_map/dot_general | solution.py:195
  311.5 3.8 %all_to_all.28 = bf16[2,16,1024]{2,1,0:T(8,128)(2,1)S(1)} all-to-all(bf16[2,16,1024]{2,1,0:T(8,128)(2,1)S(1)} %bitcast.71), channel_id=1, replica_groups=mesh['ep'=64,'tp'=2] {'tp'}, dimensions={0} | all-to-all | bytes 131072 | tf_op jit(solution)/shard_map/all_to_all | solution.py:37
  315.2 8.6 %all-to-all-start.3 = ((bf16[64,2,1024]{2,1,0:T(2,128)(2,1)}), bf16[64,2,1024]{2,1,0:T(2,128)(2,1)S(1)}, u32[]{:S(2)}, u32[]{:S(2)}) async-start(bf16[64,2,1024]{2,1,0:T(2,128)(2,1)} %convert_element_type.114), calls=%async_computation.3 | async-start | bytes 524288 | tf_op jit(solution)/shard_map/all_to_all | solution.py:181
  324.0 10.8 %all-to-all-done.3 = bf16[64,2,1024]{2,1,0:T(2,128)(2,1)S(1)} async-done(((bf16[64,2,1024]{2,1,0:T(2,128)(2,1)}), bf16[64,2,1024]{2,1,0:T(2,128)(2,1)S(1)}, u32[]{:S(2)}, u32[]{:S(2)}) %all-to-all-start.3) | async-done | bytes 262176 | tf_op jit(solution)/shard_map/all_to_all | solution.py:181
  (62 shorter events, 9.6 us)
Async XLA Ops:
  7.2 92.2 %copy-start.1 = (bf16[16,2048]{1,0:T(8,128)(2,1)S(1)}, bf16[16,2048]{1,0:T(8,128)(2,1)}, u32[]{:S(2)}) copy-start(bf16[16,2048]{1,0:T(8,128)(2,1)} %param.23) | copy-start | bytes 196612
  7.2 92.2 %copy-start.8 = (f32[2048]{0:T(1024)S(1)}, f32[2048]{0:T(1024)}, u32[]{:S(2)}) copy-start(f32[2048]{0:T(1024)} %param.24) | copy-start | bytes 24580
  7.2 86.8 %all-gather.4.cloned.1.call-start = ((), (), s32[]{:S(2)}) async-start(), calls=%async_computation.5 | async-start | bytes 9052160 | tf_op jit(solution)/shard_map/all_gather | solution.py:14
  10.4 151.5 %all-gather.6.cloned.1.call-start = ((), (), s32[]{:S(2)}) async-start(), calls=%async_computation.6 | async-start | bytes 2129920 | tf_op jit(solution)/shard_map/all_gather | solution.py:150
  11.1 285.5 %all-gather.8.cloned.1.call-start = ((), (), s32[]{:S(2)}) async-start(), calls=%async_computation.7 | async-start | bytes 25559040 | tf_op jit(solution)/shard_map/all_gather | solution.py:14
  97.1 8.4 %copy-start.5 = (f32[16,4]{0,1:T(4,128)}, f32[16,4]{0,1:T(4,128)S(1)}, u32[]{:S(2)}) copy-start(f32[16,4]{0,1:T(4,128)S(1)} %get-tuple-element.6) | copy-start | bytes 772
  108.7 2.0 copy-start
  110.7 1.3 copy-start.4
  110.7 57.5 %copy-start.2 = (f32[2048]{0:T(1024)S(1)}, f32[2048]{0:T(1024)}, u32[]{:S(2)}) copy-start(f32[2048]{0:T(1024)} %param.36) | copy-start | bytes 24580
  302.2 21.6 %copy-start.6 = (f32[2048]{0:T(1024)S(1)}, f32[2048]{0:T(1024)}, u32[]{:S(2)}) copy-start(f32[2048]{0:T(1024)} %param.45) | copy-start | bytes 24580
  302.2 21.7 %copy-start.3 = (s32[16,4]{0,1:T(4,128)S(1)}, s32[16,4]{0,1:T(4,128)}, u32[]{:S(2)}) copy-start(s32[16,4]{0,1:T(4,128)} %param.37) | copy-start | bytes 772
  302.2 21.7 %copy-start.7 = (f32[16,4]{0,1:T(4,128)S(1)}, f32[16,4]{0,1:T(4,128)}, u32[]{:S(2)}) copy-start(f32[16,4]{0,1:T(4,128)} %param.38) | copy-start | bytes 772
  315.2 19.5 %all-to-all-start.3 = ((bf16[64,2,1024]{2,1,0:T(2,128)(2,1)}), bf16[64,2,1024]{2,1,0:T(2,128)(2,1)S(1)}, u32[]{:S(2)}, u32[]{:S(2)}) async-start(bf16[64,2,1024]{2,1,0:T(2,128)(2,1)} %convert_element_type.114), calls=%async_computation.3 | async-start | bytes 524288 | tf_op jit(solution)/shard_map/all_to_all | solution.py:181
Sparse Core Ops, SparseCore 0:
  11.3 82.5 all-gather.3
  96.8 64.9 all-gather.5
  164.6 131.9 all-gather.7
where the time goes:
time: 343 us; the launch traced here: 342 us
  waiting for transfers between devices  231 us (67%)
  matrix products  39.2 us (11%)
  blocking collectives  34.3 us (10%)
  between operations  14 us (4%)
  starting transfers between devices  8.72 us (3%)
  other arithmetic  7.55 us (2%)
  local copies, waits for them, and re-layouts  7.16 us (2%)
    all_gather x2, waiting for transfers between devices, in_one_piece(): whole = lax.all_gather(both, axis, axis=dim, tiled=True)  170 us
    all_gather x1, waiting for transfers between devices, body(): lax.all_gather(mix_weight, 'ep', axis=1, tiled=True)  49.8 us
    all_to_all x1, blocking collectives, body(): lax.all_to_all(outgoing, 'ep', split_axis=0, concat_axis=0, tiled=True)  22.5 us
    dot_general x6, matrix products, body(): jnp.dot(normed, piece, preferred_element_type=jnp.float32)  11.2 us
    all_to_all x1, waiting for transfers between devices, body(): lax.all_to_all(halves.reshape(ep_count, count, part_width).astype(jnp.bfl...  10.8 us
    dot_general x1, matrix products, body(): total = jnp.dot(activity, down_piece, preferred_element_type=jnp.float32)  9.18 us
    all_to_all x1, starting transfers between devices, body(): lax.all_to_all(halves.reshape(ep_count, count, part_width).astype(jnp.bfl...  8.6 us
    all_to_all x2, blocking collectives, sent_and_summed(): lax.all_to_all(cut_along(shard, dim, devices), axis, 0, 0, tiled=True)  7.95 us
  transfers between devices with their start and end apart: 4, of which 4 were waited for; matrix products, arithmetic and copies ran while one was open for 10% of the time, Pallas kernels for 0%

commit v1 on v0

--- a/solution.py
+++ b/solution.py
@@ -6,6 +6,12 @@
 norm_eps = 1e-05
 clamp_limit = 7.0
 sigmoid_slope = 1.702
+
+
+def tiled_gather(x, axis, dim):
+    size = lax.axis_size(axis)
+    repeats = [size if d == dim else 1 for d in range(x.ndim)]
+    return lax.all_to_all(jnp.tile(x, repeats), axis, split_axis=dim, concat_axis=dim, tiled=True)
 
 
 def in_one_piece(arrays, axis, dim, along):
@@ -146,9 +152,7 @@
     )
     gated, memory_new, stab_new = memory_step(projected, forget_bias, memory, stabilizer, head_gain)
     partial_value = jnp.dot(
-        gated,
-        lax.all_gather(mix_weight, "ep", axis=1, tiled=True),
-        preferred_element_type=jnp.float32,
+        gated, tiled_gather(mix_weight, "ep", 1), preferred_element_type=jnp.float32
     )
     attended = taken_together(round_half(partial_value).astype(jnp.bfloat16), "tp").astype(
         jnp.float32

time: 343 us -> 295 us (0.86)
  waiting for transfers between devices: 231 us -> 169 us
  starting transfers between devices: 8.72 us -> 20.2 us
  blocking collectives: 34.3 us -> 38.1 us
    all_gather x1 -> x0, waiting for transfers between devices: 49.8 us -> none  [body(): lax.all_gather(mix_weight, 'ep', axis=1, tiled=True)]
    all_gather x2, waiting for transfers between devices: 170 us -> 158 us  [in_one_piece(): whole = lax.all_gather(both, axis, axis=dim, tiled=True)]
    all_to_all x0 -> x1, starting transfers between devices: none -> 11.5 us  [tiled_gather(): lax.all_to_all(jnp.tile(x, repeats), axis, split_axis=dim, concat_axis=di...]
    all_to_all x1, blocking collectives: 22.5 us -> 26.4 us  [body(): lax.all_to_all(outgoing, 'ep', split_axis=0, concat_axis=0, tiled=True)]
  transfers between devices with their start and end apart: 4 -> 4, of which waited for: 4 -> 3; matrix products, arithmetic and copies ran while one was open for 10% -> 11% of each run, Pallas kernels for 0% -> 0%
where the time goes in v1:
time: 295 us; the launch traced here: 294 us
  waiting for transfers between devices  169 us (57%)
  blocking collectives  38.1 us (13%)
  matrix products  37 us (13%)
  starting transfers between devices  20.2 us (7%)
  between operations  14.4 us (5%)
  local copies, waits for them, and re-layouts  9.45 us (3%)
  other arithmetic  6.15 us (2%)
    all_gather x2, waiting for transfers between devices, in_one_piece(): whole = lax.all_gather(both, axis, axis=dim, tiled=True)  158 us
    all_to_all x1, blocking collectives, body(): lax.all_to_all(outgoing, 'ep', split_axis=0, concat_axis=0, tiled=True)  26.4 us
    all_to_all x1, starting transfers between devices, tiled_gather(): lax.all_to_all(jnp.tile(x, repeats), axis, split_axis=dim, concat_axis=di...  11.5 us
    dot_general x6, matrix products, body(): jnp.dot(normed, piece, preferred_element_type=jnp.float32)  11 us
    all_to_all x1, waiting for transfers between devices, body(): lax.all_to_all(halves.reshape(ep_count, count, part_width).astype(jnp.bfl...  10.8 us
    dot_general x1, matrix products, body(): total = jnp.dot(activity, down_piece, preferred_element_type=jnp.float32)  9.19 us
    all_to_all x1, starting transfers between devices, body(): lax.all_to_all(halves.reshape(ep_count, count, part_width).astype(jnp.bfl...  8.6 us
    all_to_all x2, blocking collectives, sent_and_summed(): lax.all_to_all(cut_along(shard, dim, devices), axis, 0, 0, tiled=True)  7.95 us
  transfers between devices with their start and end apart: 4, of which 3 were waited for; matrix products, arithmetic and copies ran while one was open for 11% of the time, Pallas kernels for 0%

profile of v1, /device:TPU:0, one launch (start us, length us, event | category | flops | bytes accessed | tf_op | source)
XLA Modules:
  0.0 294.3 jit_solution(6559463762706027675)
XLA Ops:
  8.8 1.5 concatenate.6
  10.4 1.8 pad_maximum_fusion
  12.3 2.3 tile.2
  14.6 11.5 %all-to-all-start = ((bf16[512,64,32]{0,2,1:T(8,128)(2,1)}), bf16[512,64,32]{0,2,1:T(8,128)(2,1)S(1)}, u32[]{:S(2)}, u32[]{:S(2)}) async-start(bf16[512,64,32]{0,2,1:T(8,128)(2,1)} %tile.2), calls=%async_computation | async-start | bytes 4194304 | tf_op jit(solution)/shard_map/all_to_all | solution.py:14
  26.7 84.1 %all-gather.3.cloned.1.call-done = bf16[2048,2056]{1,0:T(8,128)(2,1)} async-done(((bf16[32,2056]{1,0:T(8,128)(2,1)}), bf16[2048,2056]{1,0:T(8,128)(2,1)}) %all-gather.3.cloned.1.call-update) | async-done | bytes 8421392 | tf_op jit(solution)/shard_map/all_gather | solution.py:20
  110.8 1.3 fusion.94
  112.1 1.7 subtract_exponential_fusion.1
  113.9 2.0 fusion.58
  116.0 2.0 fusion.67
  118.1 2.0 fusion.70
  120.1 2.0 fusion.88
  122.3 3.2 %multiply_add_fusion = f32[16,4,128,128]{3,2,1,0:T(8,128)S(1)} fusion(f32[16,4,128,128]{3,2,1,0:T(8,128)} %param.32, f32[16,4,128]{2,1,0:T(4,128)S(1)} %mul.168, f32[16,4,128]{2,1,0:T(4,128)S(1)} %broadcast_multiply_fusion, f32[16,4]{1,0:T(8,128)S(1)} %copy.59), kind=kLoop, calls=%fused_computation.12 | loop fusion | flops 3145728 | bytes 8454400 | tf_op jit(solution)/shard_map/add | solution.py:78
  125.5 2.0 copy-done
  129.6 3.8 %all_to_all.34 = bf16[2,16,2048]{2,1,0:T(8,128)(2,1)S(1)} all-to-all(bf16[2,16,2048]{2,1,0:T(8,128)(2,1)S(1)} %broadcast_in_dim.10), channel_id=1, replica_groups=mesh['ep'=64,'tp'=2] {'tp'}, dimensions={0} | all-to-all | bytes 262144 | tf_op jit(solution)/shard_map/all_to_all | solution.py:26
  134.6 26.4 %all_to_all.35 = bf16[64,2,2048]{2,1,0:T(2,128)(2,1)S(1)} all-to-all(bf16[64,2,2048]{2,1,0:T(2,128)(2,1)S(1)} %copy.63), channel_id=1, replica_groups=mesh['ep'=64,'tp'=2] {'ep'}, dimensions={0} | all-to-all | bytes 1048576 | tf_op jit(solution)/shard_map/all_to_all | solution.py:179
  161.2 3.0 %fusion.37 = f32[128,1024]{1,0:T(8,128)S(1)} fusion(bf16[128,2048]{1,0:T(8,128)(2,1)S(1)} %reshape.104, bf16[1,2048,1024]{2,1,0:T(8,128)(2,1)} %param.39), kind=kOutput, calls=%fused_computation.28 | convolution fusion | flops 537001984 | bytes 5242880 | tf_op jit(solution)/shard_map/dot_general | solution.py:92
  164.2 5.0 %fusion.12 = bf16[128,2048]{1,0:T(8,128)(2,1)S(1)} fusion(bf16[1,1024,2048]{2,1,0:T(8,128)(2,1)} %param.41, f32[128,1024]{1,0:T(8,128)S(1)} %fusion.37, bf16[128,2048]{1,0:T(8,128)(2,1)S(1)} %reshape.104, bf16[1,2048,1024]{2,1,0:T(8,128)(2,1)} %param.40), kind=kOutput, calls=%fused_computation.13 | convolution fusion | flops 1075183616 | bytes 9961472 | tf_op jit(solution)/shard_map/dot_general | solution.py:95
  169.3 4.2 %all_to_all.36 = bf16[2,128,1024]{2,1,0:T(8,128)(2,1)S(1)} all-to-all(bf16[2,128,1024]{2,1,0:T(8,128)(2,1)S(1)} %bitcast.69), channel_id=1, replica_groups=mesh['ep'=64,'tp'=2] {'tp'}, dimensions={0} | all-to-all | bytes 1048576 | tf_op jit(solution)/shard_map/all_to_all | solution.py:43
  174.4 74.0 %all-gather.5.cloned.1.call-done = bf16[2048,6144]{1,0:T(8,128)(2,1)} async-done(((bf16[32,6144]{1,0:T(8,128)(2,1)}), bf16[2048,6144]{1,0:T(8,128)(2,1)}) %all-gather.5.cloned.1.call-update) | async-done | bytes 25165840 | tf_op jit(solution)/shard_map/all_gather | solution.py:20
  248.4 5.6 %fusion.4 = f32[16,2048]{1,0:T(8,128)S(1)} fusion(bf16[16,2048]{1,0:T(8,128)(2,1)S(1)} %multiply_convert_fusion, bf16[2048,6144]{1,0:T(8,128)(2,1)} %all-gather.5.cloned.1.call-done), kind=kOutput, calls=%fused_computation.4 | convolution fusion | flops 134217728 | bytes 8585216 | tf_op jit(solution)/shard_map/td,fd->tf/dot_general | solution.py:194
  254.0 9.2 %fusion.21 = bf16[16,2048]{1,0:T(8,128)(2,1)S(1)} fusion(bf16[2048,6144]{1,0:T(8,128)(2,1)} %all-gather.5.cloned.1.call-done, bf16[16,2048]{1,0:T(8,128)(2,1)S(1)} %multiply_convert_fusion, f32[16,2048]{1,0:T(8,128)S(1)} %fusion.4), kind=kOutput, calls=%fused_computation.17 | convolution fusion | flops 268664832 | bytes 17039360 | tf_op jit(solution)/shard_map/dot_general | solution.py:199
  263.2 3.8 %all_to_all.37 = bf16[2,16,1024]{2,1,0:T(8,128)(2,1)S(1)} all-to-all(bf16[2,16,1024]{2,1,0:T(8,128)(2,1)S(1)} %bitcast.73), channel_id=1, replica_groups=mesh['ep'=64,'tp'=2] {'tp'}, dimensions={0} | all-to-all | bytes 131072 | tf_op jit(solution)/shard_map/all_to_all | solution.py:43
  267.0 8.6 %all-to-all-start.4 = ((bf16[64,2,1024]{2,1,0:T(2,128)(2,1)}), bf16[64,2,1024]{2,1,0:T(2,128)(2,1)S(1)}, u32[]{:S(2)}, u32[]{:S(2)}) async-start(bf16[64,2,1024]{2,1,0:T(2,128)(2,1)} %convert_element_type.114), calls=%async_computation.4 | async-start | bytes 524288 | tf_op jit(solution)/shard_map/all_to_all | solution.py:185
  275.8 10.8 %all-to-all-done.4 = bf16[64,2,1024]{2,1,0:T(2,128)(2,1)S(1)} async-done(((bf16[64,2,1024]{2,1,0:T(2,128)(2,1)}), bf16[64,2,1024]{2,1,0:T(2,128)(2,1)S(1)}, u32[]{:S(2)}, u32[]{:S(2)}) %all-to-all-start.4) | async-done | bytes 262176 | tf_op jit(solution)/shard_map/all_to_all | solution.py:185
  (66 shorter events, 7.9 us)
Async XLA Ops:
  7.2 19.0 %copy-start.3 = (s32[16,4]{0,1:T(4,128)S(1)}, s32[16,4]{0,1:T(4,128)}, u32[]{:S(2)}) copy-start(s32[16,4]{0,1:T(4,128)} %param.37) | copy-start | bytes 772
  7.2 19.4 %copy-start.1 = (bf16[16,2048]{1,0:T(8,128)(2,1)S(1)}, bf16[16,2048]{1,0:T(8,128)(2,1)}, u32[]{:S(2)}) copy-start(bf16[16,2048]{1,0:T(8,128)(2,1)} %param.23) | copy-start | bytes 196612
  7.2 103.7 %copy-start.8 = (f32[2048]{0:T(1024)S(1)}, f32[2048]{0:T(1024)}, u32[]{:S(2)}) copy-start(f32[2048]{0:T(1024)} %param.24) | copy-start | bytes 24580
  7.2 103.6 %all-gather.3.cloned.1.call-start = ((), (), s32[]{:S(2)}) async-start(), calls=%async_computation.6 | async-start | bytes 9052160 | tf_op jit(solution)/shard_map/all_gather | solution.py:20
  10.4 101.8 %copy-start.9 = (f32[16,4]{0,1:T(4,128)S(1)}, f32[16,4]{0,1:T(4,128)}, u32[]{:S(2)}) copy-start(f32[16,4]{0,1:T(4,128)} %param.33) | copy-start | bytes 772
  10.4 101.8 %copy-start.10 = (f32[4]{0:T(128)S(1)}, f32[4]{0:T(128)}, u32[]{:S(2)}) copy-start(f32[4]{0:T(128)} %param.31) | copy-start | bytes 52
  10.4 238.0 %all-gather.5.cloned.1.call-start = ((), (), s32[]{:S(2)}) async-start(), calls=%async_computation.7 | async-start | bytes 25559040 | tf_op jit(solution)/shard_map/all_gather | solution.py:20
  14.6 114.3 %all-to-all-start = ((bf16[512,64,32]{0,2,1:T(8,128)(2,1)}), bf16[512,64,32]{0,2,1:T(8,128)(2,1)S(1)}, u32[]{:S(2)}, u32[]{:S(2)}) async-start(bf16[512,64,32]{0,2,1:T(8,128)(2,1)} %tile.2), calls=%async_computation | async-start | bytes 4194304 | tf_op jit(solution)/shard_map/all_to_all | solution.py:14
  113.8 8.3 %copy-start.5 = (f32[16,4]{0,1:T(4,128)}, f32[16,4]{0,1:T(4,128)S(1)}, u32[]{:S(2)}) copy-start(f32[16,4]{0,1:T(4,128)S(1)} %get-tuple-element.6) | copy-start | bytes 772
  125.5 2.0 copy-start
  127.5 1.3 copy-start.4
  127.5 6.1 %copy-start.2 = (f32[2048]{0:T(1024)S(1)}, f32[2048]{0:T(1024)}, u32[]{:S(2)}) copy-start(f32[2048]{0:T(1024)} %param.36) | copy-start | bytes 24580
  254.0 21.6 %copy-start.6 = (f32[2048]{0:T(1024)S(1)}, f32[2048]{0:T(1024)}, u32[]{:S(2)}) copy-start(f32[2048]{0:T(1024)} %param.45) | copy-start | bytes 24580
  254.0 21.6 %copy-start.7 = (f32[16,4]{0,1:T(4,128)S(1)}, f32[16,4]{0,1:T(4,128)}, u32[]{:S(2)}) copy-start(f32[16,4]{0,1:T(4,128)} %param.38) | copy-start | bytes 772
  267.0 19.5 %all-to-all-start.4 = ((bf16[64,2,1024]{2,1,0:T(2,128)(2,1)}), bf16[64,2,1024]{2,1,0:T(2,128)(2,1)S(1)}, u32[]{:S(2)}, u32[]{:S(2)}) async-start(bf16[64,2,1024]{2,1,0:T(2,128)(2,1)} %convert_element_type.114), calls=%async_computation.4 | async-start | bytes 524288 | tf_op jit(solution)/shard_map/all_to_all | solution.py:185
Sparse Core Ops, SparseCore 0:
  11.4 99.4 all-gather.2
  113.6 134.7 all-gather.4
